TPU v7x, 32 devices: a whole 2x2x4 slice. The times are simulated.
32 devices in a mesh: rep: 2 (over y), fs: 4 (over z), tp: 4 (over x, core).
Axes of the slice: x: 2, y: 2, z: 4, core: 2. Of those that a mesh axis runs over, the one named last changes fastest.
Arguments:
- stream: bfloat16 [4096, 2048], P(('rep', 'fs', 'tp')), may hold values from -6 to 6
- gain_before: float32 [2048], replicated, may hold values from 0.1 to 1.9
- gain_after: float32 [2048], replicated, may hold values from 0.1 to 1.9
- proj_gate: bfloat16 [2048, 3584], P('fs', 'tp'), may hold values from -0.125 to 0.125
- proj_lift: bfloat16 [2048, 3584], P('fs', 'tp'), may hold values from -0.125 to 0.125
- proj_down: bfloat16 [3584, 2048], P('tp', 'fs'), may hold values from -0.09375 to 0.09375
- mixer_gain: float32 [2048], replicated, may hold values from 0.1 to 1.9
- mixer_u: bfloat16 [2048, 2048], P('fs', 'tp'), may hold values from -0.125 to 0.125
- mixer_v: bfloat16 [2048, 2048], P('fs', 'tp'), may hold values from -1 to 1
- layer_gain: float32 [2048], P('tp'), may hold values from 0.1 to 1.9
- layer_shift: float32 [2048], P('tp'), may hold values from -3 to 3
- spatial: bfloat16 [16, 128, 128], P('tp'), may hold values from -0.5 to 0.5
- spatial_shift: float32 [16, 128], P('tp'), may hold values from 0.2 to 2
- mixer_down: bfloat16 [2048, 2048], P('tp', 'fs'), may hold values from -0.125 to 0.125
Outputs:
- result: bfloat16 [4096, 2048], P(('rep', 'fs', 'tp'))
All inputs are finite; a program needn't handle non-finite values.
Results may differ from a plain program's by a relative error of at most 0.017.
Values may be sent and summed in bfloat16 or wider, within the bound.
A program may use at most 128 MiB of HBM per device.

v0:
```python
import jax
import jax.numpy as jnp
from jax import lax
from jax.sharding import PartitionSpec as P

GROUP_DIM = 128
SPAN = 128
A = 2048
norm_epsilon = 1e-06
layer_epsilon = 1e-05


def norm_rows(row_block, scale_gain):
    widened = row_block.astype(jnp.float32)
    factor = lax.rsqrt(jnp.mean(widened * widened, axis=1, keepdims=True) + norm_epsilon)
    return (widened * factor * scale_gain).astype(jnp.bfloat16)


def gathered_norm(stream_rows, scale_gain):
    gathered = lax.all_gather(stream_rows, "tp", axis=0, tiled=True)
    return norm_rows(gathered, scale_gain)


def pair_adder(normed, pieces):
    return (
        jnp.dot(normed, pieces[0], preferred_element_type=jnp.float32),
        jnp.dot(normed, pieces[1], preferred_element_type=jnp.float32),
    )


def activate(gate_vals, lift_vals):
    return (jax.nn.silu(gate_vals) * lift_vals).astype(jnp.bfloat16)


def half_again(stream_rows, scale_gain, proj_gate, proj_lift, proj_down):
    normed = gathered_norm(stream_rows, scale_gain)
    gate_vals, lift_vals = pair_adder(
        normed,
        (
            lax.all_gather(proj_gate, "fs", axis=0, tiled=True),
            lax.all_gather(proj_lift, "fs", axis=0, tiled=True),
        ),
    )
    hidden = activate(gate_vals, lift_vals)
    partial_value = jnp.dot(
        hidden,
        lax.all_gather(proj_down, "fs", axis=1, tiled=True),
        preferred_element_type=jnp.float32,
    )
    summed = lax.psum_scatter(
        partial_value.astype(jnp.bfloat16), "tp", scatter_dimension=0, tiled=True
    ).astype(jnp.float32)
    return (stream_rows.astype(jnp.float32) + 0.5 * summed).astype(jnp.bfloat16)


def token_mixer(
    stream_rows,
    mixer_gain,
    mixer_u,
    mixer_v,
    layer_gain,
    layer_shift,
    spatial,
    spatial_shift,
    mixer_down,
):
    gathered = lax.all_gather(stream_rows, "tp", axis=0, tiled=True)
    normed = norm_rows(gathered, mixer_gain)
    seq_tokens = normed.shape[0]
    u_vals, v_vals = pair_adder(
        normed,
        (
            lax.all_gather(mixer_u, "fs", axis=0, tiled=True),
            lax.all_gather(mixer_v, "fs", axis=0, tiled=True),
        ),
    )
    lifted = jax.nn.gelu(v_vals)
    moments = lax.psum((jnp.sum(lifted, axis=1), jnp.sum(lifted * lifted, axis=1)), "tp")
    centre = moments[0] / A
    spread = moments[1] / A - centre * centre
    normed_v = (
        (lifted - centre[:, None]) * lax.rsqrt(spread[:, None] + layer_epsilon) * layer_gain
        + layer_shift
    ).astype(jnp.bfloat16)
    groups_here = spatial.shape[0]
    blocked = normed_v.reshape(seq_tokens // SPAN, SPAN, groups_here, GROUP_DIM)
    causal = jnp.tril(jnp.ones((SPAN, SPAN), dtype=bool))
    masked = jnp.where(causal[None], spatial, jnp.zeros((), jnp.bfloat16))
    mixed_v = jnp.einsum("gts,bsgd->btgd", masked, blocked, preferred_element_type=jnp.float32)
    mixed_v = mixed_v + spatial_shift.T[None, :, :, None]
    gated = (jax.nn.gelu(u_vals) * mixed_v.reshape(seq_tokens, groups_here * GROUP_DIM)).astype(
        jnp.bfloat16
    )
    partial_value = jnp.dot(
        gated,
        lax.all_gather(mixer_down, "fs", axis=1, tiled=True),
        preferred_element_type=jnp.float32,
    )
    summed = lax.psum_scatter(
        partial_value.astype(jnp.bfloat16), "tp", scatter_dimension=0, tiled=True
    ).astype(jnp.float32)
    return (stream_rows.astype(jnp.float32) + summed).astype(jnp.bfloat16)


def body(
    stream,
    gain_before,
    gain_after,
    proj_gate,
    proj_lift,
    proj_down,
    mixer_gain,
    mixer_u,
    mixer_v,
    layer_gain,
    layer_shift,
    spatial,
    spatial_shift,
    mixer_down,
):
    first = half_again(stream, gain_before, proj_gate, proj_lift, proj_down)
    second = token_mixer(
        first,
        mixer_gain,
        mixer_u,
        mixer_v,
        layer_gain,
        layer_shift,
        spatial,
        spatial_shift,
        mixer_down,
    )
    result = half_again(second, gain_after, proj_gate, proj_lift, proj_down)
    return result


def solution(mesh):
    placed = (
        P(("rep", "fs", "tp"), None),
        P(),
        P(),
        P("fs", "tp"),
        P("fs", "tp"),
        P("tp", "fs"),
        P(),
        P("fs", "tp"),
        P("fs", "tp"),
        P("tp"),
        P("tp"),
        P("tp", None, None),
        P("tp", None),
        P("tp", "fs"),
    )
    return jax.shard_map(
        body, mesh=mesh, in_specs=placed, out_specs=P(("rep", "fs", "tp"), None), check_vma=False
    )
```

profile of v0, /device:TPU:0, one launch (start us, length us, event | category | flops | bytes accessed | tf_op | source)
XLA Modules:
  0.0 575.2 jit_solution(15976335767558670113)
XLA Ops:
  6.5 0.0 all-gather.10.cloned.1.call-start
  6.5 0.7 all-gather.10.cloned.1.call-update
  7.3 0.0 all-gather.12.cloned.1.call-start
  7.3 0.7 all-gather.12.cloned.1.call-update
  8.0 0.0 copy-start.10
  8.0 0.0 all-gather.14.cloned.1.call-start
  8.1 0.7 all-gather.14.cloned.1.call-update
  8.8 0.0 all-gather.16.cloned.1.call-start
  8.8 0.5 all-gather.16.cloned.1.call-update
  9.3 0.0 reduce-scatter.4.cloned.1.call-start
  9.4 24.8 %all-gather.10.cloned.1.call-done = bf16[512,2048]{1,0:T(8,128)(2,1)} async-done(((bf16[128,2048]{1,0:T(8,128)(2,1)}), bf16[512,2048]{1,0:T(8,128)(2,1)}) %all-gather.10.cloned.1.call-update) | async-done | bytes 2097168 | tf_op jit(solution)/shard_map/all_gather | solution.py:20
  34.2 2.2 fusion
  36.4 71.5 %all-gather.12.cloned.1.call-done = bf16[2048,896]{1,0:T(8,128)(2,1)} async-done(((bf16[512,896]{1,0:T(8,128)(2,1)}), bf16[2048,896]{1,0:T(8,128)(2,1)}) %all-gather.12.cloned.1.call-update) | async-done | bytes 3670032 | tf_op jit(solution)/shard_map/all_gather | solution.py:40
  107.9 0.0 copy-done.10
  107.9 0.0 copy-done.4
  107.9 5.6 fusion.42
  113.5 66.6 %all-gather.14.cloned.1.call-done = bf16[2048,896]{1,0:T(8,128)(2,1)} async-done(((bf16[512,896]{1,0:T(8,128)(2,1)}), bf16[2048,896]{1,0:T(8,128)(2,1)}) %all-gather.14.cloned.1.call-update) | async-done | bytes 3670032 | tf_op jit(solution)/shard_map/all_gather | solution.py:41
  180.2 72.1 %all-gather.16.cloned.1.call-done = bf16[896,2048]{1,0:T(8,128)(2,1)} async-done(((bf16[896,512]{1,0:T(8,128)(2,1)}), bf16[896,2048]{1,0:T(8,128)(2,1)}) %all-gather.16.cloned.1.call-update) | async-done | bytes 3670032 | tf_op jit(solution)/shard_map/all_gather | solution.py:47
  252.3 9.7 %convolution_convert_fusion.1 = bf16[512,2048]{1,0:T(8,128)(2,1)} fusion(bf16[896,2048]{1,0:T(8,128)(2,1)} %all-gather.16.cloned.1.call-done, f32[512,896]{1,0:T(8,128)} %fusion.42, bf16[2048,896]{1,0:T(8,128)(2,1)} %all-gather.14.cloned.1.call-done, bf16[512,2048]{1,0:T(8,128)(2,1)S(1)} %copy-done.4, f32[2048]{0:T(1024)S(1)} %copy-done.10, ...), kind=kOutput, calls=%fused_computation.16 | convolution fusion | flops 3766091776 | bytes 13379584 | tf_op jit(solution)/shard_map/dot_general | solution.py:45
  262.0 0.0 reduce-scatter.4.cloned.1.call-update
  262.0 0.0 all-gather.18.cloned.1.call-start
  262.0 29.9 %reduce-scatter.4.cloned.1.call-done = bf16[128,2048]{1,0:T(8,128)(2,1)} async-done(((bf16[512,2048]{1,0:T(8,128)(2,1)}), bf16[128,2048]{1,0:T(8,128)(2,1)}) %reduce-scatter.4.cloned.1.call-update) | async-done | bytes 524304 | tf_op jit(solution)/shard_map/reduce_scatter | solution.py:50
  291.9 0.0 copy-done.2
  291.9 2.0 add_convert_fusion.3
  293.9 0.0 all-gather.18.cloned.1.call-update
  293.9 0.0 all-gather.22.cloned.1.call-start
  294.0 0.7 all-gather.22.cloned.1.call-update
  294.7 0.0 all-gather.20.cloned.1.call-start
  294.7 0.7 all-gather.20.cloned.1.call-update
  295.4 0.0 all-gather.24.cloned.1.call-start
  295.5 0.7 all-gather.24.cloned.1.call-update
  296.2 0.0 reduce-scatter.6.cloned.1.call-start
  296.2 20.4 %all-gather.18.cloned.1.call-done = bf16[512,2048]{1,0:T(8,128)(2,1)} async-done(((bf16[128,2048]{1,0:T(8,128)(2,1)}), bf16[512,2048]{1,0:T(8,128)(2,1)}) %all-gather.18.cloned.1.call-update) | async-done | bytes 2097168 | tf_op jit(solution)/shard_map/all_gather | solution.py:67
  316.6 2.2 fusion.3
  318.9 0.0 copy-start.7
  318.9 0.0 copy-start.8
  318.9 45.0 %all-gather.22.cloned.1.call-done = bf16[2048,512]{1,0:T(8,128)(2,1)} async-done(((bf16[512,512]{1,0:T(8,128)(2,1)}), bf16[2048,512]{1,0:T(8,128)(2,1)}) %all-gather.22.cloned.1.call-update) | async-done | bytes 2097168 | tf_op jit(solution)/shard_map/all_gather | solution.py:74
  363.9 0.0 copy-done.11
  363.9 0.0 copy-done.3
  363.9 4.1 fusion.60
  368.0 6.5 %all-reduce = (f32[512]{0:T(512)S(1)}, f32[512]{0:T(512)S(1)}) all-reduce(f32[512]{0:T(512)S(1)} %get-tuple-element.6, f32[512]{0:T(512)S(1)} %get-tuple-element.5), channel_id=1, replica_groups=mesh['rep'=2,'fs'=4,'tp'=4] {'tp'}, use_global_device_ids=true, to_apply=%region_6.7 | all-reduce | flops 1024 | bytes 8192 | tf_op jit(solution)/shard_map/psum | solution.py:78
  374.6 1.5 add_convert_fusion.2
  376.0 0.9 reshape.47
  377.0 0.0 copy-done.9
  377.0 1.4 fusion.9
  378.4 1.3 copy.21
  379.7 30.2 %all-gather.20.cloned.1.call-done = bf16[2048,512]{1,0:T(8,128)(2,1)} async-done(((bf16[512,512]{1,0:T(8,128)(2,1)}), bf16[2048,512]{1,0:T(8,128)(2,1)}) %all-gather.20.cloned.1.call-update) | async-done | bytes 2097168 | tf_op jit(solution)/shard_map/all_gather | solution.py:73
  409.9 46.1 %all-gather.24.cloned.1.call-done = bf16[512,2048]{1,0:T(8,128)(2,1)} async-done(((bf16[512,512]{1,0:T(8,128)(2,1)}), bf16[512,2048]{1,0:T(8,128)(2,1)}) %all-gather.24.cloned.1.call-update) | async-done | bytes 2097168 | tf_op jit(solution)/shard_map/all_gather | solution.py:96
  456.0 6.5 %convolution_convert_fusion.2 = bf16[512,2048]{1,0:T(8,128)(2,1)} fusion(bf16[512,2048]{1,0:T(8,128)(2,1)} %all-gather.24.cloned.1.call-done, f32[64,8,4,128]{3,2,1,0:T(4,128)} %bitcast.25, bf16[2048,512]{1,0:T(8,128)(2,1)} %all-gather.20.cloned.1.call-done, bf16[512,2048]{1,0:T(8,128)(2,1)S(1)} %copy-done.3, f32[2048]{0:T(1024)S(1)} %copy-done.11, ...), kind=kOutput, calls=%fused_computation.17 | convolution fusion | flops 2155347968 | bytes 9447424 | tf_op jit(solution)/shard_map/dot_general | solution.py:94
  462.5 0.0 reduce-scatter.6.cloned.1.call-update
  462.5 0.0 copy-start.12
  462.5 0.0 all-gather.26.cloned.1.call-start
  462.6 30.1 %reduce-scatter.6.cloned.1.call-done = bf16[128,2048]{1,0:T(8,128)(2,1)} async-done(((bf16[512,2048]{1,0:T(8,128)(2,1)}), bf16[128,2048]{1,0:T(8,128)(2,1)}) %reduce-scatter.6.cloned.1.call-update) | async-done | bytes 524304 | tf_op jit(solution)/shard_map/reduce_scatter | solution.py:99
  492.7 2.0 add_convert_fusion.1
  494.6 0.0 all-gather.26.cloned.1.call-update
  494.6 0.2 reduce-scatter.8.cloned.1.call-start
  494.9 22.5 %all-gather.26.cloned.1.call-done = bf16[512,2048]{1,0:T(8,128)(2,1)} async-done(((bf16[128,2048]{1,0:T(8,128)(2,1)}), bf16[512,2048]{1,0:T(8,128)(2,1)}) %all-gather.26.cloned.1.call-update) | async-done | bytes 2097168 | tf_op jit(solution)/shard_map/all_gather | solution.py:20
  517.4 2.2 fusion.6
  519.6 0.0 copy-done.12
  519.6 5.7 fusion.28
  525.3 9.7 %convolution_convert_fusion = bf16[512,2048]{1,0:T(8,128)(2,1)} fusion(bf16[896,2048]{1,0:T(8,128)(2,1)} %all-gather.16.cloned.1.call-done, f32[512,896]{1,0:T(8,128)} %fusion.28, bf16[2048,896]{1,0:T(8,128)(2,1)} %all-gather.14.cloned.1.call-done, bf16[512,2048]{1,0:T(8,128)(2,1)S(1)} %copy-done.5, f32[2048]{0:T(1024)S(1)} %copy-done.12, ...), kind=kOutput, calls=%fused_computation.15 | convolution fusion | flops 3766091776 | bytes 13379584 | tf_op jit(solution)/shard_map/dot_general | solution.py:45
  535.0 0.0 reduce-scatter.8.cloned.1.call-update
  535.0 31.3 %reduce-scatter.8.cloned.1.call-done = bf16[128,2048]{1,0:T(8,128)(2,1)} async-done(((bf16[512,2048]{1,0:T(8,128)(2,1)}), bf16[128,2048]{1,0:T(8,128)(2,1)}) %reduce-scatter.8.cloned.1.call-update) | async-done | bytes 524304 | tf_op jit(solution)/shard_map/reduce_scatter | solution.py:50
  566.4 2.0 add_convert_fusion
  (20 shorter events, 0.1 us)
Async XLA Ops:
  6.5 27.7 %all-gather.10.cloned.1.call-start = ((), (), s32[]{:S(2)}) async-start(), calls=%async_computation.3 | async-start | bytes 2621440 | tf_op jit(solution)/shard_map/all_gather | solution.py:20
  7.3 100.6 %all-gather.12.cloned.1.call-start = ((), (), s32[]{:S(2)}) async-start(), calls=%async_computation.4 | async-start | bytes 4587520 | tf_op jit(solution)/shard_map/all_gather | solution.py:40
  8.0 99.9 %copy-start.10 = (f32[2048]{0:T(1024)S(1)}, f32[2048]{0:T(1024)}, u32[]{:S(2)}) copy-start(f32[2048]{0:T(1024)} %param.15) | copy-start | bytes 24580
  8.0 172.2 %all-gather.14.cloned.1.call-start = ((), (), s32[]{:S(2)}) async-start(), calls=%async_computation.5 | async-start | bytes 4587520 | tf_op jit(solution)/shard_map/all_gather | solution.py:41
  8.8 243.5 %all-gather.16.cloned.1.call-start = ((), (), s32[]{:S(2)}) async-start(), calls=%async_computation.6 | async-start | bytes 4587520 | tf_op jit(solution)/shard_map/all_gather | solution.py:47
  9.3 282.6 %reduce-scatter.4.cloned.1.call-start = ((), (), s32[]{:S(2)}) async-start(), calls=%async_computation.7 | async-start | bytes 2621440 | tf_op jit(solution)/shard_map/reduce_scatter | solution.py:50
  34.2 73.7 %copy-start.4 = (bf16[512,2048]{1,0:T(8,128)(2,1)S(1)}, bf16[512,2048]{1,0:T(8,128)(2,1)}, u32[]{:S(2)}) copy-start(bf16[512,2048]{1,0:T(8,128)(2,1)} %all-gather.10.cloned.1.call-done) | copy-start | bytes 6291460
  262.0 29.9 %copy-start.2 = (bf16[128,2048]{1,0:T(8,128)(2,1)S(1)}, bf16[128,2048]{1,0:T(8,128)(2,1)}, u32[]{:S(2)}) copy-start(bf16[128,2048]{1,0:T(8,128)(2,1)} %param.14) | copy-start | bytes 1572868
  262.0 54.6 %all-gather.18.cloned.1.call-start = ((), (), s32[]{:S(2)}) async-start(), calls=%async_computation.8 | async-start | bytes 2621440 | tf_op jit(solution)/shard_map/all_gather | solution.py:67
  293.9 70.0 %copy-start.11 = (f32[2048]{0:T(1024)S(1)}, f32[2048]{0:T(1024)}, u32[]{:S(2)}) copy-start(f32[2048]{0:T(1024)} %param.20) | copy-start | bytes 24580
  293.9 70.0 %all-gather.22.cloned.1.call-start = ((), (), s32[]{:S(2)}) async-start(), calls=%async_computation.10 | async-start | bytes 2621440 | tf_op jit(solution)/shard_map/all_gather | solution.py:74
  294.7 115.3 %all-gather.20.cloned.1.call-start = ((), (), s32[]{:S(2)}) async-start(), calls=%async_computation.9 | async-start | bytes 2621440 | tf_op jit(solution)/shard_map/all_gather | solution.py:73
  295.4 160.6 %all-gather.24.cloned.1.call-start = ((), (), s32[]{:S(2)}) async-start(), calls=%async_computation.11 | async-start | bytes 2621440 | tf_op jit(solution)/shard_map/all_gather | solution.py:96
  296.2 196.5 %reduce-scatter.6.cloned.1.call-start = ((), (), s32[]{:S(2)}) async-start(), calls=%async_computation.12 | async-start | bytes 2621440 | tf_op jit(solution)/shard_map/reduce_scatter | solution.py:99
  316.6 47.3 %copy-start.3 = (bf16[512,2048]{1,0:T(8,128)(2,1)S(1)}, bf16[512,2048]{1,0:T(8,128)(2,1)}, u32[]{:S(2)}) copy-start(bf16[512,2048]{1,0:T(8,128)(2,1)} %all-gather.18.cloned.1.call-done) | copy-start | bytes 6291460
  318.9 55.7 %copy-start.7 = (f32[512]{0:T(512)S(1)}, f32[512]{0:T(512)}, u32[]{:S(2)}) copy-start(f32[512]{0:T(512)} %param.24) | copy-start | bytes 6148
  318.9 55.7 %copy-start.8 = (f32[512]{0:T(512)S(1)}, f32[512]{0:T(512)}, u32[]{:S(2)}) copy-start(f32[512]{0:T(512)} %param.23) | copy-start | bytes 6148
  368.0 8.9 %copy-start.6 = (bf16[4,128,128]{2,1,0:T(8,128)(2,1)S(1)}, bf16[4,128,128]{2,1,0:T(8,128)(2,1)}, u32[]{:S(2)}) copy-start(bf16[4,128,128]{2,1,0:T(8,128)(2,1)} %param.25) | copy-start | bytes 393220
  368.0 8.9 %copy-start.9 = (f32[4,128]{1,0:T(4,128)S(1)}, f32[4,128]{1,0:T(4,128)}, u32[]{:S(2)}) copy-start(f32[4,128]{1,0:T(4,128)} %param.26) | copy-start | bytes 6148
  462.5 30.2 %copy-start = (bf16[128,2048]{1,0:T(8,128)(2,1)S(1)}, bf16[128,2048]{1,0:T(8,128)(2,1)}, u32[]{:S(2)}) copy-start(bf16[128,2048]{1,0:T(8,128)(2,1)} %add_convert_fusion.3) | copy-start | bytes 1572868
  462.5 57.1 %copy-start.12 = (f32[2048]{0:T(1024)S(1)}, f32[2048]{0:T(1024)}, u32[]{:S(2)}) copy-start(f32[2048]{0:T(1024)} %param.16) | copy-start | bytes 24580
  462.5 54.8 %all-gather.26.cloned.1.call-start = ((), (), s32[]{:S(2)}) async-start(), calls=%async_computation.13 | async-start | bytes 2621440 | tf_op jit(solution)/shard_map/all_gather | solution.py:20
  494.6 71.7 %reduce-scatter.8.cloned.1.call-start = ((), (), s32[]{:S(2)}) async-start(), calls=%async_computation.14 | async-start | bytes 2621440 | tf_op jit(solution)/shard_map/reduce_scatter | solution.py:50
  517.4 2.2 copy-start.5
  535.0 31.4 %copy-start.1 = (bf16[128,2048]{1,0:T(8,128)(2,1)S(1)}, bf16[128,2048]{1,0:T(8,128)(2,1)}, u32[]{:S(2)}) copy-start(bf16[128,2048]{1,0:T(8,128)(2,1)} %add_convert_fusion.1) | copy-start | bytes 1572868
Sparse Core Ops, SparseCore 0:
  8.9 25.2 all-gather.9
  35.8 72.0 all-gather.11
  109.5 70.6 all-gather.13
  181.6 70.6 all-gather.15
  262.1 29.7 reduce-scatter.3
  294.1 22.5 all-gather.17
  318.2 45.6 all-gather.21
  365.5 44.4 all-gather.19
  411.5 44.4 all-gather.23
  462.6 29.9 reduce-scatter.5
  494.8 22.5 all-gather.25
  535.1 31.1 reduce-scatter.7
where the time goes:
time: 576 us; the launch traced here: 575 us
  waiting for transfers between devices  495 us (86%)
  matrix products  42.7 us (7%)
  other arithmetic  14.1 us (2%)
  between operations  13.7 us (2%)
  blocking collectives  6.51 us (1%)
    all_gather x1, waiting for transfers between devices, half_again(): lax.all_gather(proj_down, 'fs', axis=1, tiled=True)  72.1 us
    all_gather x1, waiting for transfers between devices, half_again(): lax.all_gather(proj_gate, 'fs', axis=0, tiled=True)  71.5 us
    all_gather x1, waiting for transfers between devices, half_again(): lax.all_gather(proj_lift, 'fs', axis=0, tiled=True)  66.6 us
    reduce_scatter x2, waiting for transfers between devices, half_again(): lax.psum_scatter(partial_value.astype(jnp.bfloat16), 'tp', scatter_dimens...  61.2 us
    all_gather x2, waiting for transfers between devices, gathered_norm(): gathered = lax.all_gather(stream_rows, 'tp', axis=0, tiled=True)  47.3 us
    all_gather x1, waiting for transfers between devices, token_mixer(): lax.all_gather(mixer_down, 'fs', axis=1, tiled=True)  46.1 us
    all_gather x1, waiting for transfers between devices, token_mixer(): lax.all_gather(mixer_v, 'fs', axis=0, tiled=True)  45 us
    all_gather x1, waiting for transfers between devices, token_mixer(): lax.all_gather(mixer_u, 'fs', axis=0, tiled=True)  30.2 us
  transfers between devices with their start and end apart: 12, of which 12 were waited for; matrix products, arithmetic and copies ran while one was open for 3% of the time, Pallas kernels for 0%

commit v1 on v0

--- a/solution.py
+++ b/solution.py
@@ -93,7 +93,7 @@
     )
     partial_value = jnp.dot(
         gated,
-        lax.all_gather(mixer_down, "fs", axis=1, tiled=True),
+        jnp.concatenate(lax.all_gather(mixer_down, "fs"), axis=1),
         preferred_element_type=jnp.float32,
     )
     summed = lax.psum_scatter(

time: 576 us -> 575 us (level)
  transfers between devices with their start and end apart: 12 -> 12, of which waited for: 12 -> 12; matrix products, arithmetic and copies ran while one was open for 3% -> 4% of each run, Pallas kernels for 0% -> 0%
where the time goes in v1:
time: 575 us; the launch traced here: 574 us
  waiting for transfers between devices  490 us (85%)
  matrix products  42.7 us (7%)
  other arithmetic  14.1 us (2%)
  between operations  13.7 us (2%)
  blocking collectives  6.5 us (1%)
  local copies, waits for them, and re-layouts  6.48 us (1%)
    all_gather x1, waiting for transfers between devices, half_again(): lax.all_gather(proj_down, 'fs', axis=1, tiled=True)  72.1 us
    all_gather x1, waiting for transfers between devices, half_again(): lax.all_gather(proj_gate, 'fs', axis=0, tiled=True)  71.5 us
    all_gather x1, waiting for transfers between devices, half_again(): lax.all_gather(proj_lift, 'fs', axis=0, tiled=True)  66.6 us
    reduce_scatter x2, waiting for transfers between devices, half_again(): lax.psum_scatter(partial_value.astype(jnp.bfloat16), 'tp', scatter_dimens...  60.6 us
    all_gather x2, waiting for transfers between devices, gathered_norm(): gathered = lax.all_gather(stream_rows, 'tp', axis=0, tiled=True)  47.3 us
    all_gather x1, waiting for transfers between devices, token_mixer(): lax.all_gather(mixer_v, 'fs', axis=0, tiled=True)  45 us
    all_gather x1, waiting for transfers between devices, token_mixer(): lax.all_gather(mixer_down, 'fs')  43.5 us
    all_gather x1, waiting for transfers between devices, token_mixer(): lax.all_gather(mixer_u, 'fs', axis=0, tiled=True)  30.3 us
  transfers between devices with their start and end apart: 12, of which 12 were waited for; matrix products, arithmetic and copies ran while one was open for 4% of the time, Pallas kernels for 0%

profile of v1, /device:TPU:0, one launch (start us, length us, event | category | flops | bytes accessed | tf_op | source)
XLA Modules:
  0.0 574.4 jit_solution(12445985912097838420)
XLA Ops:
  6.5 0.0 all-gather.11.cloned.1.call-start
  6.5 0.7 all-gather.11.cloned.1.call-update
  7.3 0.0 all-gather.13.cloned.1.call-start
  7.3 0.7 all-gather.13.cloned.1.call-update
  8.0 0.0 copy-start.10
  8.0 0.0 all-gather.15.cloned.1.call-start
  8.1 0.7 all-gather.15.cloned.1.call-update
  8.8 0.0 all-gather.17.cloned.1.call-start
  8.8 0.5 all-gather.17.cloned.1.call-update
  9.3 0.0 reduce-scatter.4.cloned.1.call-start
  9.4 24.8 %all-gather.11.cloned.1.call-done = bf16[512,2048]{1,0:T(8,128)(2,1)} async-done(((bf16[128,2048]{1,0:T(8,128)(2,1)}), bf16[512,2048]{1,0:T(8,128)(2,1)}) %all-gather.11.cloned.1.call-update) | async-done | bytes 2097168 | tf_op jit(solution)/shard_map/all_gather | solution.py:20
  34.2 2.2 fusion
  36.4 71.5 %all-gather.13.cloned.1.call-done = bf16[2048,896]{1,0:T(8,128)(2,1)} async-done(((bf16[512,896]{1,0:T(8,128)(2,1)}), bf16[2048,896]{1,0:T(8,128)(2,1)}) %all-gather.13.cloned.1.call-update) | async-done | bytes 3670032 | tf_op jit(solution)/shard_map/all_gather | solution.py:40
  107.9 0.0 copy-done.10
  107.9 0.0 copy-done.4
  107.9 5.6 fusion.42
  113.5 66.6 %all-gather.15.cloned.1.call-done = bf16[2048,896]{1,0:T(8,128)(2,1)} async-done(((bf16[512,896]{1,0:T(8,128)(2,1)}), bf16[2048,896]{1,0:T(8,128)(2,1)}) %all-gather.15.cloned.1.call-update) | async-done | bytes 3670032 | tf_op jit(solution)/shard_map/all_gather | solution.py:41
  180.2 72.1 %all-gather.17.cloned.1.call-done = bf16[896,2048]{1,0:T(8,128)(2,1)} async-done(((bf16[896,512]{1,0:T(8,128)(2,1)}), bf16[896,2048]{1,0:T(8,128)(2,1)}) %all-gather.17.cloned.1.call-update) | async-done | bytes 3670032 | tf_op jit(solution)/shard_map/all_gather | solution.py:47
  252.3 9.7 %convolution_convert_fusion.1 = bf16[512,2048]{1,0:T(8,128)(2,1)} fusion(bf16[896,2048]{1,0:T(8,128)(2,1)} %all-gather.17.cloned.1.call-done, f32[512,896]{1,0:T(8,128)} %fusion.42, bf16[2048,896]{1,0:T(8,128)(2,1)} %all-gather.15.cloned.1.call-done, bf16[512,2048]{1,0:T(8,128)(2,1)S(1)} %copy-done.4, f32[2048]{0:T(1024)S(1)} %copy-done.10, ...), kind=kOutput, calls=%fused_computation.16 | convolution fusion | flops 3766091776 | bytes 13379584 | tf_op jit(solution)/shard_map/dot_general | solution.py:45
  262.0 0.0 reduce-scatter.4.cloned.1.call-update
  262.0 0.0 all-gather.27.cloned.1.call-start
  262.0 0.5 all-gather.27.cloned.1.call-update
  262.6 0.0 all-gather.19.cloned.1.call-start
  262.6 29.3 %reduce-scatter.4.cloned.1.call-done = bf16[128,2048]{1,0:T(8,128)(2,1)} async-done(((bf16[512,2048]{1,0:T(8,128)(2,1)}), bf16[128,2048]{1,0:T(8,128)(2,1)}) %reduce-scatter.4.cloned.1.call-update) | async-done | bytes 524304 | tf_op jit(solution)/shard_map/reduce_scatter | solution.py:50
  291.9 0.0 copy-done.2
  291.9 2.0 add_convert_fusion.3
  293.9 0.0 all-gather.19.cloned.1.call-update
  293.9 0.0 all-gather.23.cloned.1.call-start
  294.0 0.7 all-gather.23.cloned.1.call-update
  294.7 0.0 all-gather.21.cloned.1.call-start
  294.7 0.7 all-gather.21.cloned.1.call-update
  295.4 0.0 reduce-scatter.6.cloned.1.call-start
  295.5 43.5 %all-gather.27.cloned.1.call-done = bf16[2048,512]{1,0:T(8,128)(2,1)} async-done(((bf16[512,512]{1,0:T(8,128)(2,1)}), bf16[2048,512]{1,0:T(8,128)(2,1)}) %all-gather.27.cloned.1.call-update) | async-done | bytes 2097168 | tf_op jit(solution)/shard_map/all_gather | solution.py:96
  339.0 4.1 copy.36
  343.1 18.8 %all-gather.19.cloned.1.call-done = bf16[512,2048]{1,0:T(8,128)(2,1)} async-done(((bf16[128,2048]{1,0:T(8,128)(2,1)}), bf16[512,2048]{1,0:T(8,128)(2,1)}) %all-gather.19.cloned.1.call-update) | async-done | bytes 2097168 | tf_op jit(solution)/shard_map/all_gather | solution.py:67
  362.0 2.2 fusion.3
  364.2 0.0 copy-start.7
  364.2 0.0 copy-start.8
  364.2 45.0 %all-gather.23.cloned.1.call-done = bf16[2048,512]{1,0:T(8,128)(2,1)} async-done(((bf16[512,512]{1,0:T(8,128)(2,1)}), bf16[2048,512]{1,0:T(8,128)(2,1)}) %all-gather.23.cloned.1.call-update) | async-done | bytes 2097168 | tf_op jit(solution)/shard_map/all_gather | solution.py:74
  409.2 0.0 copy-done.11
  409.2 0.0 copy-done.3
  409.2 4.1 fusion.60
  413.4 6.5 %all-reduce = (f32[512]{0:T(512)S(1)}, f32[512]{0:T(512)S(1)}) all-reduce(f32[512]{0:T(512)S(1)} %get-tuple-element.6, f32[512]{0:T(512)S(1)} %get-tuple-element.5), channel_id=1, replica_groups=mesh['rep'=2,'fs'=4,'tp'=4] {'tp'}, use_global_device_ids=true, to_apply=%region_6.7 | all-reduce | flops 1024 | bytes 8192 | tf_op jit(solution)/shard_map/psum | solution.py:78
  419.9 1.5 add_convert_fusion.2
  421.4 0.9 reshape.53
  422.3 1.4 fusion.9
  423.7 1.3 copy.35
  425.0 30.3 %all-gather.21.cloned.1.call-done = bf16[2048,512]{1,0:T(8,128)(2,1)} async-done(((bf16[512,512]{1,0:T(8,128)(2,1)}), bf16[2048,512]{1,0:T(8,128)(2,1)}) %all-gather.21.cloned.1.call-update) | async-done | bytes 2097168 | tf_op jit(solution)/shard_map/all_gather | solution.py:73
  455.3 6.5 %convolution_convert_fusion.2 = bf16[512,2048]{1,0:T(8,128)(2,1)} fusion(bf16[512,2048]{0,1:T(8,128)(2,1)} %bitcast.29, f32[64,8,4,128]{3,2,1,0:T(4,128)} %bitcast.31, bf16[2048,512]{1,0:T(8,128)(2,1)} %all-gather.21.cloned.1.call-done, bf16[512,2048]{1,0:T(8,128)(2,1)S(1)} %copy-done.3, f32[2048]{0:T(1024)S(1)} %copy-done.11, f32[512]{0:T(512)S(1)} %add_rsqrt_fusion.2), kind=kOutput, calls=%fused_computation.17 | convolution fusion | flops 2155347968 | bytes 9447424 | tf_op jit(solution)/shard_map/dot_general | solution.py:94
  461.8 0.0 reduce-scatter.6.cloned.1.call-update
  461.8 0.0 copy-start.12
  461.8 0.0 all-gather.25.cloned.1.call-start
  461.8 30.1 %reduce-scatter.6.cloned.1.call-done = bf16[128,2048]{1,0:T(8,128)(2,1)} async-done(((bf16[512,2048]{1,0:T(8,128)(2,1)}), bf16[128,2048]{1,0:T(8,128)(2,1)}) %reduce-scatter.6.cloned.1.call-update) | async-done | bytes 524304 | tf_op jit(solution)/shard_map/reduce_scatter | solution.py:99
  491.9 2.0 add_convert_fusion.1
  493.9 0.0 all-gather.25.cloned.1.call-update
  493.9 0.2 reduce-scatter.8.cloned.1.call-start
  494.1 22.5 %all-gather.25.cloned.1.call-done = bf16[512,2048]{1,0:T(8,128)(2,1)} async-done(((bf16[128,2048]{1,0:T(8,128)(2,1)}), bf16[512,2048]{1,0:T(8,128)(2,1)}) %all-gather.25.cloned.1.call-update) | async-done | bytes 2097168 | tf_op jit(solution)/shard_map/all_gather | solution.py:20
  516.6 2.2 fusion.6
  518.8 0.0 copy-done.12
  518.9 5.7 fusion.28
  524.6 9.7 %convolution_convert_fusion = bf16[512,2048]{1,0:T(8,128)(2,1)} fusion(bf16[896,2048]{1,0:T(8,128)(2,1)} %all-gather.17.cloned.1.call-done, f32[512,896]{1,0:T(8,128)} %fusion.28, bf16[2048,896]{1,0:T(8,128)(2,1)} %all-gather.15.cloned.1.call-done, bf16[512,2048]{1,0:T(8,128)(2,1)S(1)} %copy-done.5, f32[2048]{0:T(1024)S(1)} %copy-done.12, ...), kind=kOutput, calls=%fused_computation.15 | convolution fusion | flops 3766091776 | bytes 13379584 | tf_op jit(solution)/shard_map/dot_general | solution.py:45
  534.2 0.0 reduce-scatter.8.cloned.1.call-update
  534.3 31.3 %reduce-scatter.8.cloned.1.call-done = bf16[128,2048]{1,0:T(8,128)(2,1)} async-done(((bf16[512,2048]{1,0:T(8,128)(2,1)}), bf16[128,2048]{1,0:T(8,128)(2,1)}) %reduce-scatter.8.cloned.1.call-update) | async-done | bytes 524304 | tf_op jit(solution)/shard_map/reduce_scatter | solution.py:50
  565.6 2.0 add_convert_fusion
  (21 shorter events, 0.1 us)
Async XLA Ops:
  6.5 27.7 %all-gather.11.cloned.1.call-start = ((), (), s32[]{:S(2)}) async-start(), calls=%async_computation.3 | async-start | bytes 2621440 | tf_op jit(solution)/shard_map/all_gather | solution.py:20
  7.3 100.6 %all-gather.13.cloned.1.call-start = ((), (), s32[]{:S(2)}) async-start(), calls=%async_computation.4 | async-start | bytes 4587520 | tf_op jit(solution)/shard_map/all_gather | solution.py:40
  8.0 99.9 %copy-start.10 = (f32[2048]{0:T(1024)S(1)}, f32[2048]{0:T(1024)}, u32[]{:S(2)}) copy-start(f32[2048]{0:T(1024)} %param.15) | copy-start | bytes 24580
  8.0 172.2 %all-gather.15.cloned.1.call-start = ((), (), s32[]{:S(2)}) async-start(), calls=%async_computation.5 | async-start | bytes 4587520 | tf_op jit(solution)/shard_map/all_gather | solution.py:41
  8.8 243.5 %all-gather.17.cloned.1.call-start = ((), (), s32[]{:S(2)}) async-start(), calls=%async_computation.6 | async-start | bytes 4587520 | tf_op jit(solution)/shard_map/all_gather | solution.py:47
  9.3 282.6 %reduce-scatter.4.cloned.1.call-start = ((), (), s32[]{:S(2)}) async-start(), calls=%async_computation.7 | async-start | bytes 2621440 | tf_op jit(solution)/shard_map/reduce_scatter | solution.py:50
  34.2 73.7 %copy-start.4 = (bf16[512,2048]{1,0:T(8,128)(2,1)S(1)}, bf16[512,2048]{1,0:T(8,128)(2,1)}, u32[]{:S(2)}) copy-start(bf16[512,2048]{1,0:T(8,128)(2,1)} %all-gather.11.cloned.1.call-done) | copy-start | bytes 6291460
  262.0 29.9 %copy-start.2 = (bf16[128,2048]{1,0:T(8,128)(2,1)S(1)}, bf16[128,2048]{1,0:T(8,128)(2,1)}, u32[]{:S(2)}) copy-start(bf16[128,2048]{1,0:T(8,128)(2,1)} %param.14) | copy-start | bytes 1572868
  262.0 77.0 %all-gather.27.cloned.1.call-start = ((), (), s32[]{:S(2)}) async-start(), calls=%async_computation.14 | async-start | bytes 2621440 | tf_op jit(solution)/shard_map/all_gather | solution.py:96
  262.6 99.4 %all-gather.19.cloned.1.call-start = ((), (), s32[]{:S(2)}) async-start(), calls=%async_computation.8 | async-start | bytes 2621440 | tf_op jit(solution)/shard_map/all_gather | solution.py:67
  293.9 115.3 %all-gather.23.cloned.1.call-start = ((), (), s32[]{:S(2)}) async-start(), calls=%async_computation.10 | async-start | bytes 2621440 | tf_op jit(solution)/shard_map/all_gather | solution.py:74
  294.7 160.6 %all-gather.21.cloned.1.call-start = ((), (), s32[]{:S(2)}) async-start(), calls=%async_computation.9 | async-start | bytes 2621440 | tf_op jit(solution)/shard_map/all_gather | solution.py:73
  295.4 196.5 %reduce-scatter.6.cloned.1.call-start = ((), (), s32[]{:S(2)}) async-start(), calls=%async_computation.11 | async-start | bytes 2621440 | tf_op jit(solution)/shard_map/reduce_scatter | solution.py:99
  339.0 70.2 %copy-start.11 = (f32[2048]{0:T(1024)S(1)}, f32[2048]{0:T(1024)}, u32[]{:S(2)}) copy-start(f32[2048]{0:T(1024)} %param.20) | copy-start | bytes 24580
  362.0 47.3 %copy-start.3 = (bf16[512,2048]{1,0:T(8,128)(2,1)S(1)}, bf16[512,2048]{1,0:T(8,128)(2,1)}, u32[]{:S(2)}) copy-start(bf16[512,2048]{1,0:T(8,128)(2,1)} %all-gather.19.cloned.1.call-done) | copy-start | bytes 6291460
  364.2 55.7 %copy-start.7 = (f32[512]{0:T(512)S(1)}, f32[512]{0:T(512)}, u32[]{:S(2)}) copy-start(f32[512]{0:T(512)} %param.24) | copy-start | bytes 6148
  364.2 55.7 %copy-start.8 = (f32[512]{0:T(512)S(1)}, f32[512]{0:T(512)}, u32[]{:S(2)}) copy-start(f32[512]{0:T(512)} %param.23) | copy-start | bytes 6148
  413.4 8.9 %copy-start.6 = (bf16[4,128,128]{2,1,0:T(8,128)(2,1)S(1)}, bf16[4,128,128]{2,1,0:T(8,128)(2,1)}, u32[]{:S(2)}) copy-start(bf16[4,128,128]{2,1,0:T(8,128)(2,1)} %param.25) | copy-start | bytes 393220
  413.4 8.9 %copy-start.9 = (f32[4,128]{1,0:T(4,128)S(1)}, f32[4,128]{1,0:T(4,128)}, u32[]{:S(2)}) copy-start(f32[4,128]{1,0:T(4,128)} %param.26) | copy-start | bytes 6148
  461.8 30.2 %copy-start = (bf16[128,2048]{1,0:T(8,128)(2,1)S(1)}, bf16[128,2048]{1,0:T(8,128)(2,1)}, u32[]{:S(2)}) copy-start(bf16[128,2048]{1,0:T(8,128)(2,1)} %add_convert_fusion.3) | copy-start | bytes 1572868
  461.8 57.1 %copy-start.12 = (f32[2048]{0:T(1024)S(1)}, f32[2048]{0:T(1024)}, u32[]{:S(2)}) copy-start(f32[2048]{0:T(1024)} %param.16) | copy-start | bytes 24580
  461.8 54.8 %all-gather.25.cloned.1.call-start = ((), (), s32[]{:S(2)}) async-start(), calls=%async_computation.12 | async-start | bytes 2621440 | tf_op jit(solution)/shard_map/all_gather | solution.py:20
  493.9 71.7 %reduce-scatter.8.cloned.1.call-start = ((), (), s32[]{:S(2)}) async-start(), calls=%async_computation.13 | async-start | bytes 2621440 | tf_op jit(solution)/shard_map/reduce_scatter | solution.py:50
  516.6 2.2 copy-start.5
  534.2 31.4 %copy-start.1 = (bf16[128,2048]{1,0:T(8,128)(2,1)S(1)}, bf16[128,2048]{1,0:T(8,128)(2,1)}, u32[]{:S(2)}) copy-start(bf16[128,2048]{1,0:T(8,128)(2,1)} %add_convert_fusion.1) | copy-start | bytes 1572868
Sparse Core Ops, SparseCore 0:
  8.9 25.2 all-gather.10
  35.8 72.0 all-gather.12
  109.5 70.6 all-gather.14
  181.6 70.6 all-gather.16
  262.1 29.7 reduce-scatter.3
  293.3 45.6 all-gather.26
  340.6 21.3 all-gather.18
  363.5 45.6 all-gather.22
  410.8 44.4 all-gather.20
  461.9 29.9 reduce-scatter.5
  494.0 22.5 all-gather.24
  534.4 31.1 reduce-scatter.7
